TPU v7x, 512 devices: a 4x2x32 block of a 4x8x32 slice. The times are simulated.
512 devices in a mesh: grp: 2 (over y), sp: 32 (over z), tp: 8 (over x, core).
Axes of the slice: x: 4, y: 2, z: 32, core: 2. Of those that a mesh axis runs over, the one named last changes fastest.
The devices are a block of a 4x8x32 slice.
Arguments:
- prompt: bfloat16 [8, 6144, 2048], P('grp', 'sp'), parts along dimension 0, may hold values from -6 to 6
- w_key: bfloat16 [2048, 2048], P('sp', 'tp'), may hold values from -0.125 to 0.125
- w_value: bfloat16 [2048, 2048], P('sp', 'tp'), may hold values from -0.125 to 0.125
- query_new: bfloat16 [8, 2048], P('grp', 'tp'), parts along dimension 0, may hold values from -150 to 150
- key_new: bfloat16 [8, 2048], P('grp', 'tp'), parts along dimension 0, may hold values from -15 to 15
- value_new: bfloat16 [8, 2048], P('grp', 'tp'), parts along dimension 0, may hold values from -6 to 6
- mix_lambda: float32 [16], P('tp'), may hold values from 0.3 to 0.8
- head_gain: float32 [128], replicated, may hold values from 0.1 to 1.9
Outputs:
- key_cache: bfloat16 [64, 32, 24, 2048], P(('grp', 'sp'), None, None, 'tp'), parts along dimension 0
- value_cache: bfloat16 [64, 32, 24, 2048], P(('grp', 'sp'), None, None, 'tp'), parts along dimension 0
- first_read: bfloat16 [8, 2048], P('grp', 'tp'), parts along dimension 0
There are 2 independent parts, one for each index of `grp`. A program takes and returns all parts, laid end to end along the dimension named above; an argument that names none is the same for every part. Nothing has to cross between parts.
All inputs are finite; a program needn't handle non-finite values.
Results may differ from a plain program's by a relative error of at most 0.0065.
The roundings to bfloat16 on the way count: a program that leaves them out, or rounds other values in their place, can miss the bound.
Values may be sent and summed in bfloat16 or wider, within the bound.
No kernel may reach another device: no remote copies, remote signals or barrier semaphores. Data moves between devices by JAX's collectives and lax.ppermute only.
A program may use at most 64 MiB of HBM per device.

v0:
```python
import jax
import jax.numpy as jnp
from jax import lax
from jax.sharding import PartitionSpec as P

HALF = 64
VDIM = 128


def sent_together(arrays, axis, dim, along):
    both = jnp.concatenate(arrays, axis=along)
    result, at, finished = (lax.all_gather(both, axis, axis=dim, tiled=True), 0, [])
    for a in arrays:
        finished.append(lax.slice_in_dim(result, at, at + a.shape[along], axis=along))
        at += a.shape[along]
    return tuple(finished)


def copy_for_each(shard, axis):
    peers = lax.axis_size(axis)
    return lax.all_to_all(
        jnp.broadcast_to(shard[None], (peers, *shard.shape)), axis, 0, 0, tiled=True
    )


def collected_together(shard, axis):
    leaves = jax.tree.leaves(shard)
    order = sorted(range(len(leaves)), key=lambda k: -leaves[k].size)
    width = (1, *leaves[order[0]].shape)[-1]
    lines = [
        jnp.pad(leaves[k].reshape(-1), (0, -leaves[k].size % width)).reshape(-1, width)
        for k in order
    ]
    both, at, found = (copy_for_each(jnp.concatenate(lines), axis), 0, {})
    for k, line in zip(order, lines):
        section = both[:, at : at + len(line)].reshape(len(both), -1)
        found[k] = section[:, : leaves[k].size].reshape(-1, *leaves[k].shape)
        at += len(line)
    numbers = iter(range(len(leaves)))
    return jax.tree.map(lambda _: found[next(numbers)], shard)


def combined_pairwise(pieces, combine):
    while len(jax.tree.leaves(pieces)[0]) > 1:
        pieces = jax.vmap(combine)(
            *(jax.tree.map(lambda part: part[side::2], pieces) for side in (0, 1))
        )
    return jax.tree.map(lambda part: part[0], pieces)


def merged(shard, axis, combine):
    pieces = collected_together(shard, axis)
    return combined_pairwise(pieces, combine)


def of_everyone(shard, axis):
    return copy_for_each(shard, axis).sum(axis=0)


def project(rows, w_key, w_value):
    pieces = sent_together((w_key, w_value), "sp", 0, 1)
    keys = jnp.dot(rows, pieces[0], preferred_element_type=jnp.float32)
    values = jnp.dot(rows, pieces[1], preferred_element_type=jnp.float32)
    return (keys.astype(jnp.bfloat16), values.astype(jnp.bfloat16))


def score_maps(query, keys):
    count, span = (keys.shape[0], keys.shape[1])
    heads = query.shape[1] // (2 * HALF)
    q_parts = query.reshape(count, heads, 2, HALF)
    k_parts = keys.reshape(count, span, heads, 2, HALF)
    return jnp.einsum(
        "shmc,slhmc->shml", q_parts, k_parts, preferred_element_type=jnp.float32
    ) * HALF ** (-0.5)


def own_scores(query, fresh_key):
    count = query.shape[0]
    heads = query.shape[1] // (2 * HALF)
    q_parts = query.astype(jnp.float32).reshape(count, heads, 2, HALF)
    k_parts = fresh_key.astype(jnp.float32).reshape(count, heads, 2, HALF)
    return jnp.sum(q_parts * k_parts, axis=-1) * HALF ** (-0.5)


def finish(reads, head_gain):
    mean = jnp.mean(reads * reads, axis=-1, keepdims=True)
    normed = reads * lax.rsqrt(mean + 1e-06) * head_gain
    return normed.reshape(reads.shape[0], -1).astype(jnp.bfloat16)


def join_totals(first, second):
    top = jnp.maximum(first[0], second[0])
    return (top, first[1] * jnp.exp(first[0] - top) + second[1] * jnp.exp(second[0] - top))


def placed(part_rows, prompts, first, fill):
    base = jnp.full((prompts,) + part_rows.shape[1:], fill, jnp.float32)
    return lax.dynamic_update_slice_in_dim(base, part_rows, first, 0)


def cache_read(query_new, key_new, value_new, keys, values, mix_lambda, head_gain, first):
    count, span = (keys.shape[0], keys.shape[1])
    prompts = query_new.shape[0]
    heads = mix_lambda.shape[0]
    query = lax.dynamic_slice_in_dim(query_new, first, count, 0)
    scores = score_maps(query, keys)
    fresh_all = own_scores(query_new, key_new)
    fresh = lax.dynamic_slice_in_dim(fresh_all, first, count, 0)
    local_top = jnp.maximum(jnp.max(scores, axis=-1), fresh)
    local_total = jnp.sum(jnp.exp(scores - local_top[..., None]), axis=-1)
    top_all, cache_total = merged(
        (placed(local_top, prompts, first, -1e30), placed(local_total, prompts, first, 0.0)),
        "sp",
        join_totals,
    )
    own = jnp.exp(fresh_all - top_all)
    total_all = cache_total + own
    top = lax.dynamic_slice_in_dim(top_all, first, count, 0)
    total = lax.dynamic_slice_in_dim(total_all, first, count, 0)
    probs = jnp.exp(scores - top[..., None]) / total[..., None]
    mixed = (probs[:, :, 0] - mix_lambda[None, :, None] * probs[:, :, 1]).astype(jnp.bfloat16)
    value_parts = values.reshape(count, span, heads, VDIM)
    partial_value = jnp.einsum(
        "shl,slhv->shv", mixed, value_parts, preferred_element_type=jnp.float32
    )
    reads = of_everyone(placed(partial_value, prompts, first, 0.0), "sp")
    own_prob = own / total_all
    own_mixed = (own_prob[:, :, 0] - mix_lambda[None, :] * own_prob[:, :, 1]).astype(jnp.bfloat16)
    reads = reads + own_mixed.astype(jnp.float32)[..., None] * value_new.astype(
        jnp.float32
    ).reshape(prompts, heads, VDIM)
    return finish(reads, head_gain)


def block_read(
    query_new, key_new, value_new, key_cache, value_cache, mix_lambda, head_gain, spread
):
    blocks, sub = (key_cache.shape[1], key_cache.shape[2])
    first = lax.axis_index("sp") // spread
    keys = key_cache.reshape(1, blocks * sub, -1)
    values = value_cache.reshape(1, blocks * sub, -1)
    return cache_read(query_new, key_new, value_new, keys, values, mix_lambda, head_gain, first)


def body(prompt, w_key, w_value, query_new, key_new, value_new, mix_lambda, head_gain):
    count, piece, width = prompt.shape
    spread = lax.axis_size("sp") // count
    sub = piece // spread
    keys, values = project(prompt.reshape(count * piece, width), w_key, w_value)
    key_blocks = keys.reshape(count * spread, 1, sub, -1)
    value_blocks = values.reshape(count * spread, 1, sub, -1)
    key_cache, value_cache = (
        lax.all_to_all(key_blocks, "sp", split_axis=0, concat_axis=1, tiled=True),
        lax.all_to_all(value_blocks, "sp", split_axis=0, concat_axis=1, tiled=True),
    )
    first_read = block_read(
        query_new, key_new, value_new, key_cache, value_cache, mix_lambda, head_gain, spread
    )
    return (key_cache, value_cache, first_read)


def solution(mesh):
    placed = (
        P("grp", "sp", None),
        P("sp", "tp"),
        P("sp", "tp"),
        P("grp", "tp"),
        P("grp", "tp"),
        P("grp", "tp"),
        P("tp"),
        P(),
    )
    return jax.shard_map(
        body,
        mesh=mesh,
        in_specs=placed,
        out_specs=(
            P(("grp", "sp"), None, None, "tp"),
            P(("grp", "sp"), None, None, "tp"),
            P("grp", "tp"),
        ),
        check_vma=False,
    )
```

profile of v0, /device:TPU:34, one launch (start us, length us, event | category | flops | bytes accessed | tf_op | source)
XLA Modules:
  0.0 364.4 jit_solution(18418636442365662421)
XLA Ops:
  7.3 1.6 pad_maximum_fusion
  8.9 164.9 %all-gather.2.cloned.1.call-done = bf16[2048,512]{1,0:T(8,128)(2,1)} async-done(((bf16[64,512]{1,0:T(8,128)(2,1)}), bf16[2048,512]{1,0:T(8,128)(2,1)}) %all-gather.2.cloned.1.call-update) | async-done | bytes 2097168 | tf_op jit(solution)/shard_map/all_gather | solution.py:12
  173.8 2.3 fusion
  176.1 0.9 copy.102
  177.0 11.1 %all-to-all-start = ((bf16[32,1,24,256]{3,2,1,0:T(8,128)(2,1)}), bf16[32,1,24,256]{3,2,1,0:T(8,128)(2,1)S(1)}, u32[]{:S(2)}, u32[]{:S(2)}) async-start(bf16[32,1,24,256]{3,2,1,0:T(8,128)(2,1)} %bitcast.90), calls=%async_computation | async-start | bytes 786432 | tf_op jit(solution)/shard_map/all_to_all | solution.py:153
  188.1 3.0 fusion.1
  191.1 1.9 copy.104
  193.1 32.8 %all-to-all-done = bf16[32,1,24,256]{3,2,1,0:T(8,128)(2,1)S(1)} async-done(((bf16[32,1,24,256]{3,2,1,0:T(8,128)(2,1)}), bf16[32,1,24,256]{3,2,1,0:T(8,128)(2,1)S(1)}, u32[]{:S(2)}, u32[]{:S(2)}) %all-to-all-start) | async-done | bytes 393248 | tf_op jit(solution)/shard_map/all_to_all | solution.py:153
  225.8 5.4 %all-to-all-start.1 = ((bf16[32,1,24,256]{3,2,1,0:T(8,128)(2,1)}), bf16[32,1,24,256]{3,2,1,0:T(8,128)(2,1)}, u32[]{:S(2)}, u32[]{:S(2)}) async-start(bf16[32,1,24,256]{3,2,1,0:T(8,128)(2,1)} %bitcast.89), calls=%async_computation.1 | async-start | bytes 786432 | tf_op jit(solution)/shard_map/all_to_all | solution.py:154
  232.8 1.2 reshape.123
  234.1 1.5 fusion.4
  236.2 1.3 copy.107
  237.5 1.3 dynamic-slice_maximum_fusion
  238.9 1.3 copy.109
  240.2 1.3 copy.108
  242.1 1.3 dynamic_update_slice.11
  243.4 1.3 reshape.124
  244.8 1.4 exponential_reduce_fusion
  246.2 1.3 copy.110
  248.1 1.3 dynamic_update_slice.12
  249.4 1.3 reshape.125
  250.7 1.3 pad_maximum_fusion.1
  252.1 17.1 %all-to-all-done.1 = bf16[32,1,24,256]{3,2,1,0:T(8,128)(2,1)} async-done(((bf16[32,1,24,256]{3,2,1,0:T(8,128)(2,1)}), bf16[32,1,24,256]{3,2,1,0:T(8,128)(2,1)}, u32[]{:S(2)}, u32[]{:S(2)}) %all-to-all-start.1) | async-done | bytes 393248 | tf_op jit(solution)/shard_map/all_to_all | solution.py:154
  269.1 1.3 broadcast_in_dim.9
  270.4 5.3 %all-to-all-start.2 = ((f32[32,16,2]{1,2,0:T(2,128)}), f32[32,16,2]{1,2,0:T(2,128)}, u32[]{:S(2)}, u32[]{:S(2)}) async-start(f32[32,16,2]{1,2,0:T(2,128)} %broadcast_in_dim.9), calls=%async_computation.2 | async-start | bytes 65536 | tf_op jit(solution)/shard_map/all_to_all | solution.py:21
  275.8 1.8 reshape.126
  277.6 20.6 %all-to-all-done.2 = f32[32,16,2]{1,2,0:T(2,128)} async-done(((f32[32,16,2]{1,2,0:T(2,128)}), f32[32,16,2]{1,2,0:T(2,128)}, u32[]{:S(2)}, u32[]{:S(2)}) %all-to-all-start.2) | async-done | bytes 4128 | tf_op jit(solution)/shard_map/all_to_all | solution.py:21
  298.2 1.5 fusion.23
  299.7 1.4 copy.131
  301.1 1.5 slice.91
  302.6 1.5 slice.92
  304.1 1.4 copy.134
  305.5 1.5 slice.102
  307.0 1.5 slice.103
  308.5 1.4 copy.136
  309.9 1.4 copy.135
  311.3 1.4 copy.133
  312.7 1.4 copy.132
  314.1 0.9 multiply_add_fusion
  317.1 0.8 divide_bitcast_fusion
  318.6 1.2 fusion.6
  320.5 5.4 %all-to-all-start.3 = ((f32[32,4,2,128]{3,2,1,0:T(2,128)}), f32[32,4,2,128]{3,2,1,0:T(2,128)}, u32[]{:S(2)}, u32[]{:S(2)}) async-start(f32[32,4,2,128]{3,2,1,0:T(2,128)} %broadcast_in_dim.11), calls=%async_computation.3 | async-start | bytes 262144 | tf_op jit(solution)/shard_map/all_to_all | solution.py:21
  327.2 0.8 bitcast_convert_fusion
  328.1 24.5 %all-to-all-done.3 = f32[32,4,2,128]{3,2,1,0:T(2,128)} async-done(((f32[32,4,2,128]{3,2,1,0:T(2,128)}), f32[32,4,2,128]{3,2,1,0:T(2,128)}, u32[]{:S(2)}, u32[]{:S(2)}) %all-to-all-start.3) | async-done | bytes 131104 | tf_op jit(solution)/shard_map/all_to_all | solution.py:21
  352.6 1.0 reduce_sum.43
  353.8 1.3 fusion.12
  355.0 0.7 copy.184
  355.8 1.8 copy.185
  (37 shorter events, 8.8 us)
Async XLA Ops:
  7.2 166.6 %copy-start = (bf16[4,192,2048]{2,1,0:T(8,128)(2,1)S(1)}, bf16[4,192,2048]{2,1,0:T(8,128)(2,1)}, u32[]{:S(2)}) copy-start(bf16[4,192,2048]{2,1,0:T(8,128)(2,1)} %param.8) | copy-start | bytes 9437188
  7.2 166.6 %all-gather.2.cloned.1.call-start = ((), (), s32[]{:S(2)}) async-start(), calls=%async_computation.4 | async-start | bytes 2162688 | tf_op jit(solution)/shard_map/all_gather | solution.py:12
  177.0 48.9 %all-to-all-start = ((bf16[32,1,24,256]{3,2,1,0:T(8,128)(2,1)}), bf16[32,1,24,256]{3,2,1,0:T(8,128)(2,1)S(1)}, u32[]{:S(2)}, u32[]{:S(2)}) async-start(bf16[32,1,24,256]{3,2,1,0:T(8,128)(2,1)} %bitcast.90), calls=%async_computation | async-start | bytes 786432 | tf_op jit(solution)/shard_map/all_to_all | solution.py:153
  188.1 43.2 %copy-start.1 = (bf16[4,256]{1,0:T(4,128)(2,1)S(1)}, bf16[4,256]{1,0:T(4,128)(2,1)}, u32[]{:S(2)}) copy-start(bf16[4,256]{1,0:T(4,128)(2,1)} %param.11) | copy-start | bytes 6148
  188.1 43.8 %copy-start.2 = (bf16[4,256]{1,0:T(4,128)(2,1)S(1)}, bf16[4,256]{1,0:T(4,128)(2,1)}, u32[]{:S(2)}) copy-start(bf16[4,256]{1,0:T(4,128)(2,1)} %param.12) | copy-start | bytes 6148
  225.8 43.3 %all-to-all-start.1 = ((bf16[32,1,24,256]{3,2,1,0:T(8,128)(2,1)}), bf16[32,1,24,256]{3,2,1,0:T(8,128)(2,1)}, u32[]{:S(2)}, u32[]{:S(2)}) async-start(bf16[32,1,24,256]{3,2,1,0:T(8,128)(2,1)} %bitcast.89), calls=%async_computation.1 | async-start | bytes 786432 | tf_op jit(solution)/shard_map/all_to_all | solution.py:154
  270.4 27.7 %all-to-all-start.2 = ((f32[32,16,2]{1,2,0:T(2,128)}), f32[32,16,2]{1,2,0:T(2,128)}, u32[]{:S(2)}, u32[]{:S(2)}) async-start(f32[32,16,2]{1,2,0:T(2,128)} %broadcast_in_dim.9), calls=%async_computation.2 | async-start | bytes 65536 | tf_op jit(solution)/shard_map/all_to_all | solution.py:21
  320.5 32.1 %all-to-all-start.3 = ((f32[32,4,2,128]{3,2,1,0:T(2,128)}), f32[32,4,2,128]{3,2,1,0:T(2,128)}, u32[]{:S(2)}, u32[]{:S(2)}) async-start(f32[32,4,2,128]{3,2,1,0:T(2,128)} %broadcast_in_dim.11), calls=%async_computation.3 | async-start | bytes 262144 | tf_op jit(solution)/shard_map/all_to_all | solution.py:21
Sparse Core Ops, SparseCore 0:
  10.7 163.0 all-gather.1
where the time goes:
time: 366 us; the launch traced here: 364 us
  waiting for transfers between devices  260 us (71%)
  local copies, waits for them, and re-layouts  42 us (11%)
  starting transfers between devices  27.3 us (7%)
  between operations  14.2 us (4%)
  other arithmetic  13.2 us (4%)
  matrix products  7.87 us (2%)
    all_gather x1, waiting for transfers between devices, sent_together(): lax.all_gather(both, axis, axis=dim, tiled=True)  165 us
    all_to_all x2, waiting for transfers between devices, copy_for_each(): lax.all_to_all(jnp.broadcast_to(shard[None], (peers, *shard.shape)), axis...  45 us
    all_to_all x1, waiting for transfers between devices, body(): lax.all_to_all(key_blocks, 'sp', split_axis=0, concat_axis=1, tiled=True)  32.8 us
    all_to_all x1, waiting for transfers between devices, body(): lax.all_to_all(value_blocks, 'sp', split_axis=0, concat_axis=1, tiled=True)  17.1 us
    all_to_all x1, starting transfers between devices, body(): lax.all_to_all(key_blocks, 'sp', split_axis=0, concat_axis=1, tiled=True)  11.1 us
    unnamed x15, local copies, waits for them, and re-layouts  11 us
    all_to_all x2, starting transfers between devices, copy_for_each(): lax.all_to_all(jnp.broadcast_to(shard[None], (peers, *shard.shape)), axis...  10.7 us
  transfers between devices with their start and end apart: 5, of which 5 were waited for; matrix products, arithmetic and copies ran while one was open for 8% of the time, Pallas kernels for 0%

commit v1 on v0

--- a/solution.py
+++ b/solution.py
@@ -150,7 +150,12 @@
     key_blocks = keys.reshape(count * spread, 1, sub, -1)
     value_blocks = values.reshape(count * spread, 1, sub, -1)
     key_cache, value_cache = (
-        lax.all_to_all(key_blocks, "sp", split_axis=0, concat_axis=1, tiled=True),
+        jnp.concatenate(
+            lax.all_to_all(
+                jnp.stack(jnp.split(key_blocks, lax.axis_size("sp"), axis=0)), "sp", 0, 0
+            ),
+            axis=1,
+        ),
         lax.all_to_all(value_blocks, "sp", split_axis=0, concat_axis=1, tiled=True),
     )
     first_read = block_read(

time: 366 us -> 446 us (1.22)
  local copies, waits for them, and re-layouts: 42 us -> 120 us
    another operation x5 -> x40, local copies, waits for them, and re-layouts: 4.9 us -> 47.2 us  [the longest x35 42.3 us: body(): jnp.stack(jnp.split(key_blocks, lax.axis_size('sp'), axis=0))]
    unnamed x15 -> x46, local copies, waits for them, and re-layouts: 11 us -> 47.4 us
  transfers between devices with their start and end apart: 5 -> 5, of which waited for: 5 -> 5; matrix products, arithmetic and copies ran while one was open for 8% -> 7% of each run, Pallas kernels for 0% -> 0%
where the time goes in v1:
time: 446 us; the launch traced here: 442 us
  waiting for transfers between devices  258 us (58%)
  local copies, waits for them, and re-layouts  120 us (27%)
  starting transfers between devices  29.2 us (7%)
  between operations  14.3 us (3%)
  other arithmetic  13.2 us (3%)
  matrix products  7.87 us (2%)
    all_gather x1, waiting for transfers between devices, sent_together(): lax.all_gather(both, axis, axis=dim, tiled=True)  163 us
    unnamed x46, local copies, waits for them, and re-layouts  47.4 us
    all_to_all x2, waiting for transfers between devices, copy_for_each(): lax.all_to_all(jnp.broadcast_to(shard[None], (peers, *shard.shape)), axis...  45 us
    another operation x35, local copies, waits for them, and re-layouts, body(): jnp.stack(jnp.split(key_blocks, lax.axis_size('sp'), axis=0))  42.3 us
    all_to_all x1, waiting for transfers between devices, body(): lax.all_to_all(jnp.stack(jnp.split(key_blocks, lax.axis_size('sp'), axis=...  32.8 us
    all_to_all x1, waiting for transfers between devices, body(): lax.all_to_all(value_blocks, 'sp', split_axis=0, concat_axis=1, tiled=True)  17.1 us
    all_to_all x1, starting transfers between devices, body(): lax.all_to_all(jnp.stack(jnp.split(key_blocks, lax.axis_size('sp'), axis=...  12.9 us
    all_to_all x2, starting transfers between devices, copy_for_each(): lax.all_to_all(jnp.broadcast_to(shard[None], (peers, *shard.shape)), axis...  10.8 us
  transfers between devices with their start and end apart: 5, of which 5 were waited for; matrix products, arithmetic and copies ran while one was open for 7% of the time, Pallas kernels for 0%

profile of v1, /device:TPU:34, one launch (start us, length us, event | category | flops | bytes accessed | tf_op | source)
XLA Modules:
  0.0 442.1 jit_solution(13016711477766787242)
XLA Ops:
  7.3 1.6 pad_maximum_fusion
  8.9 163.1 %all-gather.2.cloned.1.call-done = bf16[2048,512]{1,0:T(8,128)(2,1)} async-done(((bf16[64,512]{1,0:T(8,128)(2,1)}), bf16[2048,512]{1,0:T(8,128)(2,1)}) %all-gather.2.cloned.1.call-update) | async-done | bytes 2097168 | tf_op jit(solution)/shard_map/all_gather | solution.py:12
  172.0 2.2 fusion
  176.7 1.5 copy.235
  178.2 1.5 copy.234
  179.7 1.5 copy.233
  181.2 1.5 copy.232
  182.7 1.5 copy.231
  184.3 1.5 copy.230
  185.8 1.5 copy.229
  187.3 1.5 copy.228
  188.8 1.5 copy.227
  190.3 1.5 copy.226
  191.8 1.5 copy.225
  193.3 1.5 copy.224
  197.3 1.5 copy.253
  198.8 1.5 copy.252
  200.3 1.5 copy.251
  201.8 1.5 copy.250
  203.3 1.5 copy.249
  204.9 1.5 copy.248
  206.4 1.5 copy.247
  207.9 1.5 copy.246
  209.4 1.5 copy.245
  210.9 1.5 copy.244
  212.4 1.5 copy.243
  213.9 1.5 copy.242
  252.8 12.9 %all-to-all-start = ((bf16[32,1,1,24,256]{4,3,2,1,0:T(8,128)(2,1)}), bf16[32,1,1,24,256]{4,3,2,1,0:T(8,128)(2,1)S(1)}, u32[]{:S(2)}, u32[]{:S(2)}) async-start(bf16[32,1,1,24,256]{4,3,2,1,0:T(8,128)(2,1)} %constant_dynamic-update-slice_fusion), calls=%async_computation | async-start | bytes 786432 | tf_op jit(solution)/shard_map/all_to_all | solution.py:154
  265.8 3.0 fusion.1
  268.8 1.9 copy.255
  270.7 32.8 %all-to-all-done = bf16[32,1,1,24,256]{4,3,2,1,0:T(8,128)(2,1)S(1)} async-done(((bf16[32,1,1,24,256]{4,3,2,1,0:T(8,128)(2,1)}), bf16[32,1,1,24,256]{4,3,2,1,0:T(8,128)(2,1)S(1)}, u32[]{:S(2)}, u32[]{:S(2)}) %all-to-all-start) | async-done | bytes 393248 | tf_op jit(solution)/shard_map/all_to_all | solution.py:154
  303.5 5.4 %all-to-all-start.1 = ((bf16[32,1,24,256]{3,2,1,0:T(8,128)(2,1)}), bf16[32,1,24,256]{3,2,1,0:T(8,128)(2,1)}, u32[]{:S(2)}, u32[]{:S(2)}) async-start(bf16[32,1,24,256]{3,2,1,0:T(8,128)(2,1)} %bitcast.150), calls=%async_computation.1 | async-start | bytes 786432 | tf_op jit(solution)/shard_map/all_to_all | solution.py:159
  311.7 1.5 fusion.4
  322.4 1.4 exponential_reduce_fusion
  329.7 17.1 %all-to-all-done.1 = bf16[32,1,24,256]{3,2,1,0:T(8,128)(2,1)} async-done(((bf16[32,1,24,256]{3,2,1,0:T(8,128)(2,1)}), bf16[32,1,24,256]{3,2,1,0:T(8,128)(2,1)}, u32[]{:S(2)}, u32[]{:S(2)}) %all-to-all-start.1) | async-done | bytes 393248 | tf_op jit(solution)/shard_map/all_to_all | solution.py:159
  348.1 5.4 %all-to-all-start.2 = ((f32[32,16,2]{1,2,0:T(2,128)}), f32[32,16,2]{1,2,0:T(2,128)}, u32[]{:S(2)}, u32[]{:S(2)}) async-start(f32[32,16,2]{1,2,0:T(2,128)} %broadcast_in_dim.9), calls=%async_computation.2 | async-start | bytes 65536 | tf_op jit(solution)/shard_map/all_to_all | solution.py:21
  353.5 1.8 reshape.187
  355.3 20.6 %all-to-all-done.2 = f32[32,16,2]{1,2,0:T(2,128)} async-done(((f32[32,16,2]{1,2,0:T(2,128)}), f32[32,16,2]{1,2,0:T(2,128)}, u32[]{:S(2)}, u32[]{:S(2)}) %all-to-all-start.2) | async-done | bytes 4128 | tf_op jit(solution)/shard_map/all_to_all | solution.py:21
  375.9 1.5 fusion.23
  377.4 1.4 copy.282
  378.9 1.5 slice.123
  380.3 1.5 slice.124
  381.8 1.4 copy.285
  383.2 1.5 slice.134
  384.7 1.5 slice.135
  398.2 5.4 %all-to-all-start.3 = ((f32[32,4,2,128]{3,2,1,0:T(2,128)}), f32[32,4,2,128]{3,2,1,0:T(2,128)}, u32[]{:S(2)}, u32[]{:S(2)}) async-start(f32[32,4,2,128]{3,2,1,0:T(2,128)} %broadcast_in_dim.11), calls=%async_computation.3 | async-start | bytes 262144 | tf_op jit(solution)/shard_map/all_to_all | solution.py:21
  405.8 24.5 %all-to-all-done.3 = f32[32,4,2,128]{3,2,1,0:T(2,128)} async-done(((f32[32,4,2,128]{3,2,1,0:T(2,128)}), f32[32,4,2,128]{3,2,1,0:T(2,128)}, u32[]{:S(2)}, u32[]{:S(2)}) %all-to-all-start.3) | async-done | bytes 131104 | tf_op jit(solution)/shard_map/all_to_all | solution.py:21
  433.5 1.8 copy.367
  (102 shorter events, 78.9 us)
Async XLA Ops:
  7.2 164.8 %copy-start = (bf16[4,192,2048]{2,1,0:T(8,128)(2,1)S(1)}, bf16[4,192,2048]{2,1,0:T(8,128)(2,1)}, u32[]{:S(2)}) copy-start(bf16[4,192,2048]{2,1,0:T(8,128)(2,1)} %param.8) | copy-start | bytes 9437188
  7.2 164.8 %all-gather.2.cloned.1.call-start = ((), (), s32[]{:S(2)}) async-start(), calls=%async_computation.4 | async-start | bytes 2162688 | tf_op jit(solution)/shard_map/all_gather | solution.py:12
  252.8 50.7 %all-to-all-start = ((bf16[32,1,1,24,256]{4,3,2,1,0:T(8,128)(2,1)}), bf16[32,1,1,24,256]{4,3,2,1,0:T(8,128)(2,1)S(1)}, u32[]{:S(2)}, u32[]{:S(2)}) async-start(bf16[32,1,1,24,256]{4,3,2,1,0:T(8,128)(2,1)} %constant_dynamic-update-slice_fusion), calls=%async_computation | async-start | bytes 786432 | tf_op jit(solution)/shard_map/all_to_all | solution.py:154
  265.8 43.2 %copy-start.1 = (bf16[4,256]{1,0:T(4,128)(2,1)S(1)}, bf16[4,256]{1,0:T(4,128)(2,1)}, u32[]{:S(2)}) copy-start(bf16[4,256]{1,0:T(4,128)(2,1)} %param.11) | copy-start | bytes 6148
  265.8 43.9 %copy-start.2 = (bf16[4,256]{1,0:T(4,128)(2,1)S(1)}, bf16[4,256]{1,0:T(4,128)(2,1)}, u32[]{:S(2)}) copy-start(bf16[4,256]{1,0:T(4,128)(2,1)} %param.12) | copy-start | bytes 6148
  303.5 43.3 %all-to-all-start.1 = ((bf16[32,1,24,256]{3,2,1,0:T(8,128)(2,1)}), bf16[32,1,24,256]{3,2,1,0:T(8,128)(2,1)}, u32[]{:S(2)}, u32[]{:S(2)}) async-start(bf16[32,1,24,256]{3,2,1,0:T(8,128)(2,1)} %bitcast.150), calls=%async_computation.1 | async-start | bytes 786432 | tf_op jit(solution)/shard_map/all_to_all | solution.py:159
  348.1 27.8 %all-to-all-start.2 = ((f32[32,16,2]{1,2,0:T(2,128)}), f32[32,16,2]{1,2,0:T(2,128)}, u32[]{:S(2)}, u32[]{:S(2)}) async-start(f32[32,16,2]{1,2,0:T(2,128)} %broadcast_in_dim.9), calls=%async_computation.2 | async-start | bytes 65536 | tf_op jit(solution)/shard_map/all_to_all | solution.py:21
  398.2 32.1 %all-to-all-start.3 = ((f32[32,4,2,128]{3,2,1,0:T(2,128)}), f32[32,4,2,128]{3,2,1,0:T(2,128)}, u32[]{:S(2)}, u32[]{:S(2)}) async-start(f32[32,4,2,128]{3,2,1,0:T(2,128)} %broadcast_in_dim.11), calls=%async_computation.3 | async-start | bytes 262144 | tf_op jit(solution)/shard_map/all_to_all | solution.py:21
Sparse Core Ops, SparseCore 0:
  10.7 161.2 all-gather.1
